TPU v7x, 512 devices: a whole 4x4x16 slice. The times are simulated.
512 devices in a mesh: fs: 64 (over z, y), tp: 8 (over x, core).
Axes of the slice: x: 4, y: 4, z: 16, core: 2. Of those that a mesh axis runs over, the one named last changes fastest.
Arguments:
- saved_inputs: bfloat16 [49152, 2048], P('fs'), may hold values from -16 to 16
- input_cot: bfloat16 [49152, 2048], P('fs', 'tp'), may hold values from -0.02734375 to 0.02734375
- gate_cot: bfloat16 [49152, 2048], P('fs', 'tp'), may hold values from -0.02734375 to 0.02734375
- input_master: float32 [2048, 2048], P('fs', 'tp'), may hold values from -6 to 6
- gate_master: float32 [2048, 2048], P('fs', 'tp'), may hold values from -6 to 6
- input_factor: bfloat16 [2048, 256], P('fs'), may hold values from -2 to 2
- gate_factor: bfloat16 [2048, 256], P('fs'), may hold values from -2 to 2
- input_first: float32 [256, 2048], P('fs', 'tp'), may hold values from -6 to 6
- input_second: float32 [256, 2048], P('fs', 'tp'), may hold values from 0.2 to 17
- gate_first: float32 [256, 2048], P('fs', 'tp'), may hold values from -6 to 6
- gate_second: float32 [256, 2048], P('fs', 'tp'), may hold values from 0.2 to 17
Outputs:
- input_step: float32 [2048, 2048], P('fs', 'tp')
- gate_step: float32 [2048, 2048], P('fs', 'tp')
- input_first_new: float32 [256, 2048], P('fs', 'tp')
- input_second_new: float32 [256, 2048], P('fs', 'tp')
- gate_first_new: float32 [256, 2048], P('fs', 'tp')
- gate_second_new: float32 [256, 2048], P('fs', 'tp')
- input_copy: bfloat16 [2048, 2048], P(None, 'tp')
- gate_copy: bfloat16 [2048, 2048], P(None, 'tp')
All inputs are finite; a program needn't handle non-finite values.
Results may differ from a plain program's by a relative error of at most 0.0004.
Values may be sent and summed in bfloat16 or wider, within the bound.
A program may use at most 64 MiB of HBM per device.

v0:
```python
import jax
import jax.numpy as jnp
from jax import lax
from jax.sharding import Mesh
from jax.sharding import PartitionSpec as P

D = 2048
W = 2048
FS = ("fs_0", "fs_1")
FS_TP = ("fs_0", "fs_1", "tp_0", "tp_1")
TP = ("tp_0", "tp_1")
first_decay = 0.9
second_decay = 0.9
ratio_floor = 1e-08
mean_floor = 1e-06
step_size = 0.05


def own_block(parts, axes, order):
    shape = [lax.axis_size(a) for a in axes]
    parts = parts.reshape(*shape, *parts.shape[1:])
    parts = parts.transpose(*order, *range(len(axes), parts.ndim))
    parts = parts.reshape(-1, *parts.shape[len(axes) :])
    for k in order:
        parts = lax.psum_scatter(parts, axes[k], scatter_dimension=0, tiled=True)
    return parts[0]


def split_up(shard, dim, count):
    before, after = (shard.shape[:dim], shard.shape[dim + 1 :])
    return jnp.moveaxis(shard.reshape(*before, count, -1, *after), dim, 0)


def summed_rows(shard, axes, order, dim):
    count = lax.axis_size(axes)
    return own_block(split_up(shard, dim, count), axes, order)


def sent_and_summed(shard, axis, dim):
    count = lax.axis_size(axis)
    parts = lax.all_to_all(split_up(shard, dim, count), axis, 0, 0, tiled=True)
    return jnp.sum(parts, axis=0)


def sent_together(arrays, axis, dim, along):
    widths = [a.shape[along] for a in arrays]
    both = jnp.concatenate(arrays, axis=along)
    out = sent_and_summed(both, axis, dim)
    return tuple(jnp.split(out, [sum(widths[:k]) for k in range(1, len(widths))], axis=along))


def in_one_piece(arrays, axis, dim, along):
    both = jnp.concatenate(arrays, axis=along)
    out, at, finished = (lax.all_gather(both, axis, axis=dim, tiled=True), 0, [])
    for a in arrays:
        finished.append(lax.slice_in_dim(out, at, at + a.shape[along], axis=along))
        at += a.shape[along]
    return tuple(finished)


def one_axis_at_a_time(shard, axes):
    for axis in axes:
        shard = lax.psum(shard, axis)
    return shard


def moments(low_rank, first, second):
    first_new = first_decay * first + (1.0 - first_decay) * low_rank
    second_new = second_decay * second + (1.0 - second_decay) * low_rank * low_rank
    ratio = first_new / (jnp.sqrt(second_new) + ratio_floor)
    return (first_new, second_new, ratio)


def local(
    saved_inputs,
    input_cot,
    gate_cot,
    input_master,
    gate_master,
    input_factor,
    gate_factor,
    input_first,
    input_second,
    gate_first,
    gate_second,
):
    col_width = input_cot.shape[1]
    contract = (((0,), (0,)), ((), ()))
    factor_in = input_factor.astype(jnp.float32)
    factor_gate = gate_factor.astype(jnp.float32)
    term_in = lax.dot_general(saved_inputs, input_cot, contract, preferred_element_type=jnp.float32)
    term_gate = lax.dot_general(
        saved_inputs, gate_cot, contract, preferred_element_type=jnp.float32
    )
    gradients = summed_rows(jnp.concatenate([term_in, term_gate], axis=1), FS, (1, 0), 0)
    part_in = lax.dot_general(
        factor_in, gradients[:, :col_width], contract, precision=lax.Precision.HIGHEST
    )
    part_gate = lax.dot_general(
        factor_gate, gradients[:, col_width:], contract, precision=lax.Precision.HIGHEST
    )
    low_in, low_gate = sent_together((part_in, part_gate), FS, 0, 1)
    first_in, second_in, ratio_in = moments(low_in, input_first, input_second)
    first_gate, second_gate, ratio_gate = moments(low_gate, gate_first, gate_second)
    piece_in, piece_gate = in_one_piece((ratio_in, ratio_gate), FS, 0, 1)
    dir_in = jnp.dot(factor_in, piece_in, precision=lax.Precision.HIGHEST)
    dir_gate = jnp.dot(factor_gate, piece_gate, precision=lax.Precision.HIGHEST)
    square_in, square_gate = (
        one_axis_at_a_time(jnp.sum(dir_in * dir_in), FS_TP),
        one_axis_at_a_time(jnp.sum(dir_gate * dir_gate), FS_TP),
    )
    step_in = dir_in * lax.rsqrt(square_in / (D * W) + mean_floor)
    step_gate = dir_gate * lax.rsqrt(square_gate / (D * W) + mean_floor)
    local_in = (input_master - step_size * step_in).astype(jnp.bfloat16)
    local_gate = (gate_master - step_size * step_gate).astype(jnp.bfloat16)
    copy_in, copy_gate = in_one_piece((local_in, local_gate), FS, 0, 1)
    return (step_in, step_gate, first_in, second_in, first_gate, second_gate, copy_in, copy_gate)


def solution(mesh):
    finer = Mesh(mesh.devices.reshape(16, 4, 4, 2), ("fs_0", "fs_1", "tp_0", "tp_1"))
    placed = (
        P(FS, None),
        P(FS, TP),
        P(FS, TP),
        P(FS, TP),
        P(FS, TP),
        P(FS, None),
        P(FS, None),
        P(FS, TP),
        P(FS, TP),
        P(FS, TP),
        P(FS, TP),
    )
    return jax.shard_map(
        local,
        mesh=finer,
        in_specs=placed,
        out_specs=(
            P(FS, TP),
            P(FS, TP),
            P(FS, TP),
            P(FS, TP),
            P(FS, TP),
            P(FS, TP),
            P(None, TP),
            P(None, TP),
        ),
        check_vma=False,
    )
```

profile of v0, /device:TPU:2, one launch (start us, length us, event | category | flops | bytes accessed | tf_op | source)
XLA Modules:
  0.0 511.1 jit_solution(1282623223704920424)
XLA Ops:
  7.2 0.0 reduce-scatter.3.cloned.1.call-start
  7.2 1.8 copy-done
  9.1 2.0 fusion.11
  11.1 1.0 fusion.12
  12.1 2.5 pad_maximum_fusion
  14.6 5.3 %copy.22 = f32[2048,512]{1,0:T(8,128)} copy(f32[2048,512]{0,1:T(8,128)} %pad_maximum_fusion) | data formatting | bytes 8388608 | tf_op jit(solution)/shard_map/concatenate | solution.py:95
  19.9 5.0 copy.23
  24.9 0.0 reduce-scatter.5.cloned.1.call-start
  25.0 59.1 %reduce-scatter.3.cloned.1.call-done = f32[16,32,512]{2,1,0:T(8,128)} async-done(((f32[64,32,512]{2,1,0:T(8,128)}), f32[16,32,512]{2,1,0:T(8,128)}) %reduce-scatter.3.cloned.1.call-update) | async-done | bytes 1048592 | tf_op jit(solution)/shard_map/reduce_scatter | solution.py:25
  84.1 0.0 all-gather.3.cloned.1.call-start
  84.1 73.8 %reduce-scatter.5.cloned.1.call-done = f32[1,32,512]{2,1,0:T(8,128)} async-done(((f32[16,32,512]{2,1,0:T(8,128)}), f32[1,32,512]{2,1,0:T(8,128)}) %reduce-scatter.5.cloned.1.call-update) | async-done | bytes 65552 | tf_op jit(solution)/shard_map/reduce_scatter | solution.py:25
  158.0 1.1 convolution_bitcast_fusion
  159.1 1.1 convolution_bitcast_fusion.1
  160.1 0.8 pad_maximum_fusion.1
  161.0 2.0 copy.24
  163.0 2.0 reshape.23
  165.0 35.0 %all_to_all.5 = f32[64,4,512]{2,1,0:T(4,128)} all-to-all(f32[64,4,512]{2,1,0:T(4,128)} %reshape.23), channel_id=1, replica_groups=mesh['fs_0'=16,'fs_1'=4,'tp_0'=4,'tp_1'=2] {'fs_0','fs_1'}, dimensions={0} | all-to-all | bytes 1048576 | tf_op jit(solution)/shard_map/all_to_all | solution.py:41
  200.0 1.2 reduce_sum.27
  201.2 0.6 add_divide_fusion.1
  201.8 107.3 %all-gather = f32[64,4,512]{2,1,0:T(4,128)} all-gather(f32[1,4,512]{2,1,0:T(4,128)S(1)} %maximum_bitcast_fusion), channel_id=1, replica_groups=mesh['fs_0'=16,'fs_1'=4,'tp_0'=4,'tp_1'=2] {'fs_0','fs_1'}, dimensions={0}, use_global_device_ids=true | all-gather | bytes 532480 | tf_op jit(solution)/shard_map/all_gather | solution.py:54
  309.1 2.0 reshape.25
  311.1 1.8 multiply_reduce_fusion
  312.9 1.8 multiply_reduce_fusion.1
  314.7 28.8 %all-reduce = (f32[]{:T(128)}, f32[]{:T(128)}) all-reduce(f32[]{:T(128)} %get-tuple-element.31, f32[]{:T(128)} %get-tuple-element.33), channel_id=1, replica_groups=mesh['fs_0'=16,'fs_1'=4,'tp_0'=4,'tp_1'=2] {'fs_0'}, use_global_device_ids=true, to_apply=%region_4.0 | all-reduce | flops 2 | bytes 16 | tf_op jit(solution)/shard_map/psum | solution.py:63
  343.5 10.7 %all-reduce.2 = (f32[]{:T(128)}, f32[]{:T(128)}) all-reduce(f32[]{:T(128)} %get-tuple-element.8, f32[]{:T(128)} %get-tuple-element.9), channel_id=1, replica_groups=mesh['fs_0'=16,'fs_1'=4,'tp_0'=4,'tp_1'=2] {'fs_1'}, use_global_device_ids=true, to_apply=%region_5.0 | all-reduce | flops 2 | bytes 16 | tf_op jit(solution)/shard_map/psum | solution.py:63
  354.2 9.3 %all-reduce.1 = (f32[]{:T(128)}, f32[]{:T(128)}) all-reduce(f32[]{:T(128)} %get-tuple-element.12, f32[]{:T(128)} %get-tuple-element.13), channel_id=1, replica_groups=mesh['fs_0'=16,'fs_1'=4,'tp_0'=4,'tp_1'=2] {'tp_0'}, use_global_device_ids=true, to_apply=%region_6.0 | all-reduce | flops 2 | bytes 16 | tf_op jit(solution)/shard_map/psum | solution.py:63
  363.5 3.1 all-reduce.3
  368.0 0.6 subtract_convert_fusion
  368.6 0.6 pad_maximum_fusion.2
  369.2 0.0 all-gather.3.cloned.1.call-update
  369.3 132.4 %all-gather.3.cloned.1.call-done = bf16[2048,512]{1,0:T(8,128)(2,1)} async-done(((bf16[32,512]{1,0:T(8,128)(2,1)}), bf16[2048,512]{1,0:T(8,128)(2,1)}) %all-gather.3.cloned.1.call-update) | async-done | bytes 2097168 | tf_op jit(solution)/shard_map/all_gather | solution.py:54
  501.6 3.0 fusion.10
  (22 shorter events, 0.1 us)
Async XLA Ops:
  7.2 1.9 copy-start
  7.2 3.9 copy-start.1
  7.2 76.9 %reduce-scatter.3.cloned.1.call-start = ((), (), s32[]{:S(2)}) async-start(), calls=%async_computation.3 | async-start | bytes 5242880 | tf_op jit(solution)/shard_map/reduce_scatter | solution.py:25
  24.9 133.1 %copy-start.2 = (bf16[32,256]{1,0:T(8,128)(2,1)S(1)}, bf16[32,256]{1,0:T(8,128)(2,1)}, u32[]{:S(2)}) copy-start(bf16[32,256]{1,0:T(8,128)(2,1)} %param.17) | copy-start | bytes 49156
  24.9 134.2 %copy-start.3 = (bf16[32,256]{1,0:T(8,128)(2,1)S(1)}, bf16[32,256]{1,0:T(8,128)(2,1)}, u32[]{:S(2)}) copy-start(bf16[32,256]{1,0:T(8,128)(2,1)} %param.16) | copy-start | bytes 49156
  24.9 133.0 %reduce-scatter.5.cloned.1.call-start = ((), (), s32[]{:S(2)}) async-start(), calls=%async_computation.4 | async-start | bytes 1114112 | tf_op jit(solution)/shard_map/reduce_scatter | solution.py:25
  84.1 117.1 %copy-start.6 = (f32[4,256]{1,0:T(4,128)S(1)}, f32[4,256]{1,0:T(4,128)}, u32[]{:S(2)}) copy-start(f32[4,256]{1,0:T(4,128)} %param.19) | copy-start | bytes 12292
  84.1 117.1 %copy-start.7 = (f32[4,256]{1,0:T(4,128)S(1)}, f32[4,256]{1,0:T(4,128)}, u32[]{:S(2)}) copy-start(f32[4,256]{1,0:T(4,128)} %param.18) | copy-start | bytes 12292
  84.1 117.1 %copy-start.8 = (f32[4,256]{1,0:T(4,128)S(1)}, f32[4,256]{1,0:T(4,128)}, u32[]{:S(2)}) copy-start(f32[4,256]{1,0:T(4,128)} %param.21) | copy-start | bytes 12292
  84.1 117.1 %copy-start.9 = (f32[4,256]{1,0:T(4,128)S(1)}, f32[4,256]{1,0:T(4,128)}, u32[]{:S(2)}) copy-start(f32[4,256]{1,0:T(4,128)} %param.20) | copy-start | bytes 12292
  84.1 417.5 %all-gather.3.cloned.1.call-start = ((), (), s32[]{:S(2)}) async-start(), calls=%async_computation.5 | async-start | bytes 2129920 | tf_op jit(solution)/shard_map/all_gather | solution.py:54
  161.0 207.0 %copy-start.4 = (f32[32,256]{1,0:T(8,128)S(1)}, f32[32,256]{1,0:T(8,128)}, u32[]{:S(2)}) copy-start(f32[32,256]{1,0:T(8,128)} %param.15) | copy-start | bytes 98308
  161.0 207.0 %copy-start.5 = (f32[32,256]{1,0:T(8,128)S(1)}, f32[32,256]{1,0:T(8,128)}, u32[]{:S(2)}) copy-start(f32[32,256]{1,0:T(8,128)} %param.14) | copy-start | bytes 98308
Sparse Core Ops, SparseCore 0:
  25.0 58.9 reduce-scatter.2
  86.9 71.0 reduce-scatter.4
  369.4 132.1 all-gather.2
where the time goes:
time: 512 us; the launch traced here: 511 us
  waiting for transfers between devices  265 us (52%)
  blocking collectives  194 us (38%)
  local copies, waits for them, and re-layouts  21.2 us (4%)
  between operations  15.2 us (3%)
  matrix products  8.73 us (2%)
  other arithmetic  6.31 us (1%)
    reduce_scatter x2, waiting for transfers between devices, own_block(): parts = lax.psum_scatter(parts, axes[k], scatter_dimension=0, tiled=True)  133 us
    all_gather x1, waiting for transfers between devices, in_one_piece(): lax.all_gather(both, axis, axis=dim, tiled=True)  132 us
    all_gather x1, blocking collectives, in_one_piece(): lax.all_gather(both, axis, axis=dim, tiled=True)  107 us
    psum x4, blocking collectives, one_axis_at_a_time(): shard = lax.psum(shard, axis)  51.9 us
    all_to_all x1, blocking collectives, sent_and_summed(): parts = lax.all_to_all(split_up(shard, dim, count), axis, 0, 0, tiled=True)  35 us
  transfers between devices with their start and end apart: 3, of which 3 were waited for; matrix products, arithmetic and copies ran while one was open for 0% of the time, Pallas kernels for 0%

commit v1 on v0

--- a/solution.py
+++ b/solution.py
@@ -60,7 +60,7 @@
 
 def one_axis_at_a_time(shard, axes):
     for axis in axes:
-        shard = lax.psum(shard, axis)
+        shard = jnp.sum(lax.all_gather(shard, axis), axis=0)
     return shard
 
 

time: 512 us -> 528 us (1.031)
  blocking collectives: 194 us -> 157 us
  waiting for transfers between devices: 265 us -> 285 us
  local copies, waits for them, and re-layouts: 21.2 us -> 37.7 us
  starting transfers between devices: 0.12 us -> 12.3 us
    psum x4 -> x0, blocking collectives: 51.9 us -> none  [one_axis_at_a_time(): shard = lax.psum(shard, axis)]
    unnamed x0 -> x4, blocking collectives: none -> 48.9 us
    all_to_all x1 -> x0, blocking collectives: 35 us -> none  [sent_and_summed(): parts = lax.all_to_all(split_up(shard, dim, count), axis, 0, 0, tiled=True)]
    all_to_all x0 -> x1, waiting for transfers between devices: none -> 20.2 us  [sent_and_summed(): parts = lax.all_to_all(split_up(shard, dim, count), axis, 0, 0, tiled=True)]
    unnamed x21 -> x41, local copies, waits for them, and re-layouts: 3.88 us -> 20.3 us
    all_to_all x0 -> x1, starting transfers between devices: none -> 12.2 us  [sent_and_summed(): parts = lax.all_to_all(split_up(shard, dim, count), axis, 0, 0, tiled=True)]
  transfers between devices with their start and end apart: 3 -> 4, of which waited for: 3 -> 4; matrix products, arithmetic and copies ran while one was open for 0% -> 0% of each run, Pallas kernels for 0% -> 0%
where the time goes in v1:
time: 528 us; the launch traced here: 527 us
  waiting for transfers between devices  285 us (54%)
  blocking collectives  157 us (30%)
  local copies, waits for them, and re-layouts  37.7 us (7%)
  between operations  15.3 us (3%)
  starting transfers between devices  12.3 us (2%)
  other arithmetic  11.1 us (2%)
  matrix products  8.74 us (2%)
    reduce_scatter x2, waiting for transfers between devices, own_block(): parts = lax.psum_scatter(parts, axes[k], scatter_dimension=0, tiled=True)  133 us
    all_gather x1, waiting for transfers between devices, in_one_piece(): lax.all_gather(both, axis, axis=dim, tiled=True)  132 us
    all_gather x1, blocking collectives, in_one_piece(): lax.all_gather(both, axis, axis=dim, tiled=True)  108 us
    unnamed x4, blocking collectives  48.9 us
    unnamed x41, local copies, waits for them, and re-layouts  20.3 us
    all_to_all x1, waiting for transfers between devices, sent_and_summed(): parts = lax.all_to_all(split_up(shard, dim, count), axis, 0, 0, tiled=True)  20.2 us
    all_to_all x1, starting transfers between devices, sent_and_summed(): parts = lax.all_to_all(split_up(shard, dim, count), axis, 0, 0, tiled=True)  12.2 us
  transfers between devices with their start and end apart: 4, of which 4 were waited for; matrix products, arithmetic and copies ran while one was open for 0% of the time, Pallas kernels for 0%

profile of v1, /device:TPU:2, one launch (start us, length us, event | category | flops | bytes accessed | tf_op | source)
XLA Modules:
  0.0 527.1 jit_solution(2903521578319546647)
XLA Ops:
  7.2 1.8 copy-done
  9.1 2.0 fusion.11
  12.1 2.5 pad_maximum_fusion
  14.6 5.3 %copy.22 = f32[2048,512]{1,0:T(8,128)} copy(f32[2048,512]{0,1:T(8,128)} %pad_maximum_fusion) | data formatting | bytes 8388608 | tf_op jit(solution)/shard_map/concatenate | solution.py:95
  19.9 5.0 copy.23
  25.0 59.1 %reduce-scatter.3.cloned.1.call-done = f32[16,32,512]{2,1,0:T(8,128)} async-done(((f32[64,32,512]{2,1,0:T(8,128)}), f32[16,32,512]{2,1,0:T(8,128)}) %reduce-scatter.3.cloned.1.call-update) | async-done | bytes 1048592 | tf_op jit(solution)/shard_map/reduce_scatter | solution.py:25
  84.1 73.9 %reduce-scatter.5.cloned.1.call-done = f32[1,32,512]{2,1,0:T(8,128)} async-done(((f32[16,32,512]{2,1,0:T(8,128)}), f32[1,32,512]{2,1,0:T(8,128)}) %reduce-scatter.5.cloned.1.call-update) | async-done | bytes 65552 | tf_op jit(solution)/shard_map/reduce_scatter | solution.py:25
  161.0 2.0 copy.24
  163.0 2.0 reshape.23
  165.0 12.2 %all-to-all-start = ((f32[64,4,512]{2,1,0:T(4,128)}), f32[64,4,512]{2,1,0:T(4,128)}, u32[]{:S(2)}, u32[]{:S(2)}) async-start(f32[64,4,512]{2,1,0:T(4,128)} %reshape.23), calls=%async_computation.2 | async-start | bytes 1048576 | tf_op jit(solution)/shard_map/all_to_all | solution.py:41
  177.2 1.3 dynamic-slice
  178.5 1.3 dynamic-slice.1
  179.9 20.2 %all-to-all-done = f32[64,4,512]{2,1,0:T(4,128)} async-done(((f32[64,4,512]{2,1,0:T(4,128)}), f32[64,4,512]{2,1,0:T(4,128)}, u32[]{:S(2)}, u32[]{:S(2)}) %all-to-all-start) | async-done | bytes 524320 | tf_op jit(solution)/shard_map/all_to_all | solution.py:41
  201.9 107.9 %all-gather = f32[64,4,512]{2,1,0:T(4,128)} all-gather(f32[1,4,512]{2,1,0:T(4,128)S(1)} %maximum_bitcast_fusion), channel_id=1, replica_groups=mesh['fs_0'=16,'fs_1'=4,'tp_0'=4,'tp_1'=2] {'fs_0','fs_1'}, dimensions={0}, use_global_device_ids=true | all-gather | bytes 532480 | tf_op jit(solution)/shard_map/all_gather | solution.py:54
  309.8 2.0 reshape.49
  311.8 1.8 multiply_reduce_fusion.1
  313.6 1.8 multiply_reduce_fusion
  315.4 1.4 dynamic-update-slice
  316.8 1.4 dynamic-update-slice.4
  318.2 27.5 %all-reduce.8 = (f32[16]{0:T(128)S(1)}, f32[16]{0:T(128)S(1)}) all-reduce(f32[16]{0:T(128)S(1)} %dynamic-update-slice, f32[16]{0:T(128)S(1)} %dynamic-update-slice.4), channel_id=1, replica_groups=mesh['fs_0'=16,'fs_1'=4,'tp_0'=4,'tp_1'=2] {'fs_0'}, use_global_device_ids=true, to_apply=%add | all-reduce | flops 32 | bytes 256
  346.9 1.4 dynamic-update-slice.5
  348.3 1.4 dynamic-update-slice.1
  349.8 1.3 dynamic-slice.2
  351.0 10.3 %all-reduce.10 = (f32[4]{0:T(128)S(1)}, f32[4]{0:T(128)S(1)}) all-reduce(f32[4]{0:T(128)S(1)} %dynamic-update-slice.1, f32[4]{0:T(128)S(1)} %dynamic-update-slice.5), channel_id=1, replica_groups=mesh['fs_0'=16,'fs_1'=4,'tp_0'=4,'tp_1'=2] {'fs_1'}, use_global_device_ids=true, to_apply=%add.1 | all-reduce | flops 8 | bytes 64
  362.5 1.4 dynamic-update-slice.6
  363.9 1.4 dynamic-update-slice.2
  366.6 8.6 %all-reduce.9 = (f32[4]{0:T(128)S(1)}, f32[4]{0:T(128)S(1)}) all-reduce(f32[4]{0:T(128)S(1)} %dynamic-update-slice.2, f32[4]{0:T(128)S(1)} %dynamic-update-slice.6), channel_id=1, replica_groups=mesh['fs_0'=16,'fs_1'=4,'tp_0'=4,'tp_1'=2] {'tp_0'}, use_global_device_ids=true, to_apply=%add.2 | all-reduce | flops 8 | bytes 64
  376.4 1.4 dynamic-update-slice.7
  377.9 1.4 dynamic-update-slice.3
  379.3 2.4 all-reduce.11
  385.6 132.0 %all-gather.3.cloned.1.call-done = bf16[2048,512]{1,0:T(8,128)(2,1)} async-done(((bf16[32,512]{1,0:T(8,128)(2,1)}), bf16[2048,512]{1,0:T(8,128)(2,1)}) %all-gather.3.cloned.1.call-update) | async-done | bytes 2097168 | tf_op jit(solution)/shard_map/all_gather | solution.py:54
  517.6 3.0 fusion.10
  (51 shorter events, 13.3 us)
Async XLA Ops:
  7.2 1.9 copy-start
  7.2 3.9 copy-start.1
  7.2 76.9 %reduce-scatter.3.cloned.1.call-start = ((), (), s32[]{:S(2)}) async-start(), calls=%async_computation.3 | async-start | bytes 5242880 | tf_op jit(solution)/shard_map/reduce_scatter | solution.py:25
  24.9 133.1 %copy-start.3 = (bf16[32,256]{1,0:T(8,128)(2,1)S(1)}, bf16[32,256]{1,0:T(8,128)(2,1)}, u32[]{:S(2)}) copy-start(bf16[32,256]{1,0:T(8,128)(2,1)} %param.17) | copy-start | bytes 49156
  24.9 134.2 %copy-start.2 = (bf16[32,256]{1,0:T(8,128)(2,1)S(1)}, bf16[32,256]{1,0:T(8,128)(2,1)}, u32[]{:S(2)}) copy-start(bf16[32,256]{1,0:T(8,128)(2,1)} %param.16) | copy-start | bytes 49156
  24.9 133.0 %reduce-scatter.5.cloned.1.call-start = ((), (), s32[]{:S(2)}) async-start(), calls=%async_computation.4 | async-start | bytes 1114112 | tf_op jit(solution)/shard_map/reduce_scatter | solution.py:25
  84.1 117.1 %copy-start.6 = (f32[4,256]{1,0:T(4,128)S(1)}, f32[4,256]{1,0:T(4,128)}, u32[]{:S(2)}) copy-start(f32[4,256]{1,0:T(4,128)} %param.19) | copy-start | bytes 12292
  84.1 117.1 %copy-start.7 = (f32[4,256]{1,0:T(4,128)S(1)}, f32[4,256]{1,0:T(4,128)}, u32[]{:S(2)}) copy-start(f32[4,256]{1,0:T(4,128)} %param.18) | copy-start | bytes 12292
  84.1 117.2 %copy-start.8 = (f32[4,256]{1,0:T(4,128)S(1)}, f32[4,256]{1,0:T(4,128)}, u32[]{:S(2)}) copy-start(f32[4,256]{1,0:T(4,128)} %param.21) | copy-start | bytes 12292
  84.1 117.2 %copy-start.9 = (f32[4,256]{1,0:T(4,128)S(1)}, f32[4,256]{1,0:T(4,128)}, u32[]{:S(2)}) copy-start(f32[4,256]{1,0:T(4,128)} %param.20) | copy-start | bytes 12292
  161.0 223.3 %copy-start.4 = (f32[32,256]{1,0:T(8,128)S(1)}, f32[32,256]{1,0:T(8,128)}, u32[]{:S(2)}) copy-start(f32[32,256]{1,0:T(8,128)} %param.15) | copy-start | bytes 98308
  161.0 223.3 %copy-start.5 = (f32[32,256]{1,0:T(8,128)S(1)}, f32[32,256]{1,0:T(8,128)}, u32[]{:S(2)}) copy-start(f32[32,256]{1,0:T(8,128)} %param.14) | copy-start | bytes 98308
  165.0 35.1 %all-to-all-start = ((f32[64,4,512]{2,1,0:T(4,128)}), f32[64,4,512]{2,1,0:T(4,128)}, u32[]{:S(2)}, u32[]{:S(2)}) async-start(f32[64,4,512]{2,1,0:T(4,128)} %reshape.23), calls=%async_computation.2 | async-start | bytes 1048576 | tf_op jit(solution)/shard_map/all_to_all | solution.py:41
  177.2 340.4 %all-gather.3.cloned.1.call-start = ((), (), s32[]{:S(2)}) async-start(), calls=%async_computation.5 | async-start | bytes 2129920 | tf_op jit(solution)/shard_map/all_gather | solution.py:54
Sparse Core Ops, SparseCore 0:
  25.1 58.9 reduce-scatter.2
  86.9 71.0 reduce-scatter.4
  385.7 131.8 all-gather.2
